TPU v7x, 32 devices: a whole 2x2x4 slice. The times are simulated.
32 devices in a mesh: grp: 2 (over y), tp: 4 (over z), dp: 4 (over x, core).
Axes of the slice: x: 2, y: 2, z: 4, core: 2. Of those that a mesh axis runs over, the one named last changes fastest.
Arguments:
- tokens: bfloat16 [128, 8, 2048], P('grp', None, 'dp'), parts along dimension 0, may hold values from -64 to 64
- live_counts: int32 [128], P(('grp', 'dp')), parts along dimension 0, may hold values from 1 to 8, 256 in all
- norm_gain: float32 [2, 2048], P(None, 'dp'), may hold values from 0.1 to 1.9
- w_branch: bfloat16 [2, 2048, 4096], P(None, 'dp', 'tp'), may hold values from -0.125 to 0.125
- w_silu_gate: bfloat16 [2, 2048, 4096], P(None, 'dp', 'tp'), may hold values from -0.125 to 0.125
- conv_weight: float32 [2, 4, 4096], P(None, None, 'tp'), may hold values from -3 to 3
- w_query: bfloat16 [2, 16, 256, 256], P(None, 'tp'), may hold values from -0.375 to 0.375
- w_key: bfloat16 [2, 16, 256, 256], P(None, 'tp'), may hold values from -0.375 to 0.375
- w_value: bfloat16 [2, 16, 256, 256], P(None, 'tp'), may hold values from -0.375 to 0.375
- w_input_gate: bfloat16 [2, 16, 768], P(None, 'tp'), may hold values from -0.21875 to 0.21875
- w_forget_gate: bfloat16 [2, 16, 768], P(None, 'tp'), may hold values from -0.21875 to 0.21875
- bias_input: float32 [2, 16], P(None, 'tp'), may hold values from -2 to 2
- bias_forget: float32 [2, 16], P(None, 'tp'), may hold values from -1 to 5
- out_gain: float32 [2, 16, 256], P(None, 'tp'), may hold values from 0.25 to 4
- skip_gain: float32 [2, 4096], P(None, 'tp'), may hold values from 0.25 to 4
- w_out: bfloat16 [2, 4096, 2048], P(None, 'tp', 'dp'), may hold values from -0.09375 to 0.09375
- conv_state: bfloat16 [2, 128, 3, 4096], P(None, ('grp', 'dp'), None, 'tp'), parts along dimension 1, may hold values from -6 to 6
- memory: float32 [2, 128, 16, 256, 256], P(None, ('grp', 'dp'), 'tp'), parts along dimension 1, may hold values from -0.375 to 0.375
- max_state: float32 [2, 128, 16], P(None, ('grp', 'dp'), 'tp'), parts along dimension 1, may hold values from -4 to 4
Outputs:
- out_tokens: bfloat16 [128, 8, 2048], P('grp', None, 'dp'), parts along dimension 0
- new_conv_state: bfloat16 [2, 128, 3, 4096], P(None, ('grp', 'dp'), None, 'tp'), parts along dimension 1
- new_memory: float32 [2, 128, 16, 256, 256], P(None, ('grp', 'dp'), 'tp'), parts along dimension 1
- new_max: float32 [2, 128, 16], P(None, ('grp', 'dp'), 'tp'), parts along dimension 1
There are 2 independent parts, one for each index of `grp`. A program takes and returns all parts, laid end to end along the dimension named above; an argument that names none is the same for every part. Nothing has to cross between parts.
Inputs may be any that keep to these rules, and one draw needn't show every extreme that they name: `live_counts`: each sequence has at least one live slot; within each part (each independent copy of the problem) the 64 counts sum to 256, so the whole array sums to that times the number of parts; in each part some sequence uses all 8 slots.
All inputs are finite; a program needn't handle non-finite values. No bound on the sum of `live_counts` on one device may be relied on, other than what follows from the above.
Results may differ from a plain program's by a relative error of at most 0.035.
Values may be sent and summed in bfloat16 or wider, within the bound.
A program may use at most 192 MiB of HBM per device.

v0:
```python
import jax
import jax.numpy as jnp
from jax import lax
from jax.sharding import PartitionSpec as P

D = 2048
HEAD_DIM = 256
CONV = 4
LAYERS = 2
epsilon = 1e-06
very_negative = -1e30


def recurrent_cell(
    branch,
    silu_gate,
    live_counts,
    conv_weight,
    w_query,
    w_key,
    w_value,
    w_input_gate,
    w_forget_gate,
    bias_input,
    bias_forget,
    out_gain,
    skip_gain,
    conv_state,
    memory,
    max_state,
):
    local_batch = branch.shape[0]
    steps = branch.shape[1]
    local_width = branch.shape[2]
    local_heads = w_query.shape[0]
    padded = jnp.concatenate([conv_state, branch], axis=1)
    conv_sum = jnp.zeros((local_batch, steps, local_width), jnp.float32)
    for offset in range(CONV):
        conv_sum = (
            conv_sum + padded[:, offset : offset + steps].astype(jnp.float32) * conv_weight[offset]
        )
    convolved = jax.nn.silu(conv_sum).astype(jnp.bfloat16)
    picks = live_counts[:, None] + jnp.arange(CONV - 1, dtype=jnp.int32)[None, :]
    new_conv = jnp.take_along_axis(padded, picks[:, :, None], axis=1)
    conv_heads = convolved.reshape(local_batch, steps, local_heads, HEAD_DIM)
    branch_heads = branch.reshape(local_batch, steps, local_heads, HEAD_DIM)
    queries = jnp.einsum(
        "blhd,hde->blhe", conv_heads, w_query, preferred_element_type=jnp.float32
    ).astype(jnp.bfloat16)
    key_rows = jnp.einsum(
        "blhd,hde->blhe", conv_heads, w_key, preferred_element_type=jnp.float32
    ).astype(jnp.bfloat16)
    value_rows = jnp.einsum(
        "blhd,hde->blhe", branch_heads, w_value, preferred_element_type=jnp.float32
    ).astype(jnp.bfloat16)
    joined = jnp.concatenate([queries, key_rows, value_rows], axis=-1)
    input_log = (
        jnp.einsum("blhc,hc->blh", joined, w_input_gate, preferred_element_type=jnp.float32)
        + bias_input
    )
    forget_pre = (
        jnp.einsum("blhc,hc->blh", joined, w_forget_gate, preferred_element_type=jnp.float32)
        + bias_forget
    )
    forget_log = jax.nn.log_sigmoid(forget_pre)
    positions = jnp.arange(steps, dtype=jnp.int32)
    live = positions[None, :] < live_counts[:, None]
    input_log = jnp.transpose(jnp.where(live[:, :, None], input_log, very_negative), (0, 2, 1))
    forget_log = jnp.transpose(jnp.where(live[:, :, None], forget_log, 0.0), (0, 2, 1))
    query_heads = jnp.transpose(queries.astype(jnp.float32), (0, 2, 1, 3))
    key_heads = jnp.transpose(key_rows.astype(jnp.float32), (0, 2, 1, 3)) * HEAD_DIM ** (-0.5)
    value_heads = jnp.transpose(value_rows.astype(jnp.float32), (0, 2, 1, 3))
    cumulative = jnp.cumsum(forget_log, axis=-1)
    log_weights = cumulative[..., :, None] - cumulative[..., None, :] + input_log[..., None, :]
    causal = positions[:, None] >= positions[None, :]
    log_weights = jnp.where(causal, log_weights, very_negative)
    carried = cumulative + max_state[..., None]
    stabilizer = jnp.maximum(jnp.max(log_weights, axis=-1), carried)
    weights = jnp.exp(log_weights - stabilizer[..., None])
    carried_scale = jnp.exp(carried - stabilizer)
    scores = jnp.einsum("bhtd,bhsd->bhts", query_heads, key_heads) * weights
    numerator = jnp.einsum("bhts,bhse->bhte", scores, value_heads)
    numerator = numerator + carried_scale[..., None] * jnp.einsum(
        "bhtd,bhde->bhte", query_heads, memory
    )
    centered = numerator - jnp.mean(numerator, axis=-1, keepdims=True)
    normalized = centered * lax.rsqrt(
        jnp.mean(centered * centered, axis=-1, keepdims=True) + epsilon
    )
    normalized = normalized * out_gain[None, :, None, :]
    readout = jnp.transpose(normalized, (0, 2, 1, 3)).reshape(local_batch, steps, local_width)
    new_max = stabilizer[..., -1]
    decay = jnp.exp(cumulative[..., -1] + max_state - new_max)
    update_weight = jnp.exp(cumulative[..., -1:] - cumulative + input_log - new_max[..., None])
    new_memory = decay[..., None, None] * memory + jnp.einsum(
        "bhs,bhsd,bhse->bhde", update_weight, key_heads, value_heads
    )
    mixed = (readout + skip_gain * convolved.astype(jnp.float32)) * jax.nn.silu(
        silu_gate.astype(jnp.float32)
    )
    mixed = jnp.where(live[:, :, None], mixed, 0.0).astype(jnp.bfloat16)
    return (mixed, new_conv, new_memory, new_max)


def layer_step(
    tokens,
    live_counts,
    gain,
    w_branch,
    w_silu_gate,
    conv_weight,
    w_query,
    w_key,
    w_value,
    w_input_gate,
    w_forget_gate,
    bias_input,
    bias_forget,
    out_gain,
    skip_gain,
    w_out,
    conv_state,
    memory,
    max_state,
):
    all_batch = tokens.shape[0]
    steps = tokens.shape[1]
    local_features = tokens.shape[2]
    local_width = w_branch.shape[1]
    local_batch = live_counts.shape[0]
    floats = tokens.astype(jnp.float32)
    partial_squares = jnp.sum(floats * floats, axis=-1)
    total_squares = lax.psum(partial_squares, "dp")
    normed = (floats * lax.rsqrt(total_squares / D + epsilon)[..., None] * gain).astype(
        jnp.bfloat16
    )
    rows = normed.reshape(local_batch * lax.axis_size("dp") * steps, local_features)
    first = jnp.dot(rows, w_branch, preferred_element_type=jnp.float32)
    second = jnp.dot(rows, w_silu_gate, preferred_element_type=jnp.float32)
    summed = lax.psum_scatter(
        jnp.stack([first, second], axis=1)
        .reshape(local_batch * lax.axis_size("dp"), steps, 2, local_width)
        .astype(jnp.bfloat16),
        "dp",
        scatter_dimension=0,
        tiled=True,
    ).astype(jnp.float32)
    branch = summed[:, :, 0].astype(jnp.bfloat16)
    silu_gate = summed[:, :, 1].astype(jnp.bfloat16)
    mixed, new_conv, new_memory, new_max = recurrent_cell(
        branch,
        silu_gate,
        live_counts,
        conv_weight,
        w_query,
        w_key,
        w_value,
        w_input_gate,
        w_forget_gate,
        bias_input,
        bias_forget,
        out_gain,
        skip_gain,
        conv_state,
        memory,
        max_state,
    )
    piece = lax.all_gather(mixed, "dp", axis=0, tiled=True)
    flat = piece.reshape(piece.shape[0] * steps, local_width)
    product = jnp.dot(flat, w_out, preferred_element_type=jnp.float32)
    terms = product.reshape(piece.shape[0], steps, local_features)
    flat_terms = terms.reshape(all_batch * steps, local_features)
    share = lax.psum_scatter(
        flat_terms.astype(jnp.bfloat16), "tp", scatter_dimension=0, tiled=True
    ).astype(jnp.float32)
    share_rows = share.shape[0]
    residual_rows = lax.dynamic_slice_in_dim(
        floats.reshape(all_batch * steps, local_features),
        lax.axis_index("tp") * share_rows,
        share_rows,
        0,
    )
    new_share = (residual_rows + share.astype(jnp.bfloat16).astype(jnp.float32)).astype(
        jnp.bfloat16
    )
    result = lax.all_gather(new_share, "tp", axis=0, tiled=True).reshape(
        all_batch, steps, local_features
    )
    return (result, new_conv, new_memory, new_max)


def per_device(
    tokens,
    live_counts,
    norm_gain,
    w_branch,
    w_silu_gate,
    conv_weight,
    w_query,
    w_key,
    w_value,
    w_input_gate,
    w_forget_gate,
    bias_input,
    bias_forget,
    out_gain,
    skip_gain,
    w_out,
    conv_state,
    memory,
    max_state,
):
    stream = tokens
    conv_list = []
    memory_list = []
    max_list = []
    for which_layer in range(LAYERS):
        stream, new_conv, new_memory, new_max = layer_step(
            stream,
            live_counts,
            norm_gain[which_layer],
            w_branch[which_layer],
            w_silu_gate[which_layer],
            conv_weight[which_layer],
            w_query[which_layer],
            w_key[which_layer],
            w_value[which_layer],
            w_input_gate[which_layer],
            w_forget_gate[which_layer],
            bias_input[which_layer],
            bias_forget[which_layer],
            out_gain[which_layer],
            skip_gain[which_layer],
            w_out[which_layer],
            conv_state[which_layer],
            memory[which_layer],
            max_state[which_layer],
        )
        conv_list.append(new_conv)
        memory_list.append(new_memory)
        max_list.append(new_max)
    return (stream, jnp.stack(conv_list), jnp.stack(memory_list), jnp.stack(max_list))


def solution(mesh):
    in_specs = (
        P("grp", None, "dp"),
        P(("grp", "dp")),
        P(None, "dp"),
        P(None, "dp", "tp"),
        P(None, "dp", "tp"),
        P(None, None, "tp"),
        P(None, "tp", None, None),
        P(None, "tp", None, None),
        P(None, "tp", None, None),
        P(None, "tp", None),
        P(None, "tp", None),
        P(None, "tp"),
        P(None, "tp"),
        P(None, "tp", None),
        P(None, "tp"),
        P(None, "tp", "dp"),
        P(None, ("grp", "dp"), None, "tp"),
        P(None, ("grp", "dp"), "tp", None, None),
        P(None, ("grp", "dp"), "tp"),
    )
    out_specs = (
        P("grp", None, "dp"),
        P(None, ("grp", "dp"), None, "tp"),
        P(None, ("grp", "dp"), "tp", None, None),
        P(None, ("grp", "dp"), "tp"),
    )
    return jax.shard_map(
        per_device, mesh=mesh, in_specs=in_specs, out_specs=out_specs, check_vma=False
    )
```

profile of v0, /device:TPU:0, one launch (start us, length us, event | category | flops | bytes accessed | tf_op | source)
XLA Modules:
  0.0 297.1 jit_solution(8914190688373300822)
XLA Ops:
  7.2 1.4 fusion.162
  8.7 1.2 fusion.16
  9.9 12.9 %psum.14 = f32[64,8]{1,0:T(8,128)S(1)} all-reduce(f32[64,8]{1,0:T(8,128)S(1)} %fusion.16), channel_id=1, replica_groups=mesh['grp'=2,'tp'=4,'dp'=4] {'dp'}, use_global_device_ids=true, to_apply=%region_1.0 | all-reduce | flops 512 | bytes 4096 | tf_op jit(solution)/shard_map/psum | solution.py:133
  22.8 2.1 fusion.11
  25.0 0.8 fusion.10
  26.2 2.5 copy.279
  29.5 0.6 slice_bitcast_fusion.8
  30.1 0.5 slice_bitcast_fusion.10
  30.7 0.6 slice_bitcast_fusion.11
  31.3 0.6 slice_bitcast_fusion.6
  31.9 0.6 fusion.161
  32.5 0.6 slice_bitcast_fusion.2
  33.1 0.6 slice_bitcast_fusion.3
  33.7 0.6 fusion.160
  34.3 26.1 %reduce-scatter.15.cloned.1.call-done = bf16[16,16384]{1,0:T(8,128)(2,1)} async-done(((bf16[64,16384]{1,0:T(8,128)(2,1)}), bf16[16,16384]{1,0:T(8,128)(2,1)}) %reduce-scatter.15.cloned.1.call-update) | async-done | bytes 524304
  60.5 1.4 copy.280
  62.1 0.9 reshape.308
  63.7 1.4 convolution_convert_fusion.10
  65.6 1.8 fusion.76
  67.4 1.8 fusion.77
  69.4 2.8 reduce_window_sum.17
  73.6 0.8 exponential_multiply_fusion.1
  74.4 0.8 bitcast_multiply_fusion.6
  75.2 7.0 %fusion.4 = f32[16,4,8,256]{3,2,1,0:T(8,128)S(1)} fusion(f32[2,16,4,256,256]{4,3,2,1,0:T(8,128)} %param.38, bf16[4,16,8,256]{3,2,1,0:T(8,128)(2,1)S(1)} %convolution_convert_fusion.11), kind=kOutput, calls=%fused_computation.9 | convolution fusion | flops 67108864 | bytes 9175040 | tf_op jit(solution)/shard_map/bhtd,bhde->bhte/dot_general | solution.py:83
  82.2 1.4 fusion.108
  84.3 0.5 fusion.71
  84.8 0.9 copy.214
  85.8 16.8 %all-gather.3.cloned.1.call-done = bf16[64,8,1024]{2,1,0:T(8,128)(2,1)} async-done(((bf16[16,8,1024]{2,1,0:T(8,128)(2,1)}), bf16[64,8,1024]{2,1,0:T(8,128)(2,1)}) %all-gather.3.cloned.1.call-update) | async-done | bytes 1048592 | tf_op jit(solution)/shard_map/all_gather | solution.py:168
  102.6 3.0 %convolution_convert_fusion.5 = bf16[512,512]{1,0:T(8,128)(2,1)} fusion(bf16[64,8,1024]{2,1,0:T(8,128)(2,1)} %all-gather.3.cloned.1.call-done, bf16[2,1024,512]{2,1,0:T(8,128)(2,1)} %param.36), kind=kOutput, calls=%fused_computation.29 | convolution fusion | flops 537133056 | bytes 2621440 | tf_op jit(solution)/shard_map/dot_general | solution.py:170
  105.8 21.8 %reduce-scatter.11.cloned.1.call-done = bf16[128,512]{1,0:T(8,128)(2,1)} async-done(((bf16[512,512]{1,0:T(8,128)(2,1)}), bf16[128,512]{1,0:T(8,128)(2,1)}) %reduce-scatter.11.cloned.1.call-update) | async-done | bytes 131088 | tf_op jit(solution)/shard_map/reduce_scatter | solution.py:173
  127.6 0.9 add_convert_fusion.1
  128.6 15.6 %all_gather.13 = bf16[512,512]{1,0:T(8,128)(2,1)S(1)} all-gather(bf16[128,512]{1,0:T(8,128)(2,1)S(1)} %add_convert_fusion.1), channel_id=1, replica_groups=mesh['grp'=2,'tp'=4,'dp'=4] {'tp'}, dimensions={0}, use_global_device_ids=true | all-gather | bytes 655360 | tf_op jit(solution)/shard_map/all_gather | solution.py:186
  144.4 10.3 %psum.15 = f32[64,8]{1,0:T(8,128)S(1)} all-reduce(f32[64,8]{1,0:T(8,128)S(1)} %reduce_sum.60), channel_id=1, replica_groups=mesh['grp'=2,'tp'=4,'dp'=4] {'dp'}, use_global_device_ids=true, to_apply=%region_9.10 | all-reduce | flops 512 | bytes 4096 | tf_op jit(solution)/shard_map/psum | solution.py:133
  154.8 2.0 fusion.13
  156.8 2.0 fusion.12
  159.2 2.5 copy.281
  161.8 0.6 copy-done.46
  162.4 0.7 copy.228
  163.5 28.2 %reduce-scatter.17.cloned.1.call-done = bf16[16,16384]{1,0:T(8,128)(2,1)} async-done(((bf16[64,16384]{1,0:T(8,128)(2,1)}), bf16[16,16384]{1,0:T(8,128)(2,1)}) %reduce-scatter.17.cloned.1.call-update) | async-done | bytes 524304
  191.6 1.4 copy.282
  193.0 0.7 fusion.158
  193.9 0.9 reshape.309
  195.3 1.4 convolution_convert_fusion.8
  196.8 1.4 convolution_convert_fusion.7
  198.2 1.5 convolution_convert_fusion.6
  199.8 1.8 fusion.74
  201.6 1.8 fusion.75
  203.6 2.8 reduce_window_sum.18
  207.1 7.1 %fusion = f32[16,4,8,256]{3,2,1,0:T(8,128)S(1)} fusion(f32[2,16,4,256,256]{4,3,2,1,0:T(8,128)} %param.38, bf16[4,16,8,256]{3,2,1,0:T(8,128)(2,1)} %copy-done.1), kind=kOutput, calls=%fused_computation.4 | convolution fusion | flops 67108864 | bytes 9175040 | tf_op jit(solution)/shard_map/bhtd,bhde->bhte/dot_general | solution.py:83
  214.2 1.2 gather_fusion
  215.4 1.2 gather_fusion.1
  217.1 0.8 copy.250
  218.7 1.7 bitcast_multiply_fusion.3
  220.4 1.5 fusion.109
  222.9 0.5 fusion.70
  223.4 0.9 copy.227
  224.5 0.6 pad_maximum_fusion.12
  225.1 10.8 %fusion.3 = f32[1,16,4,256,256]{4,3,2,1,0:T(8,128)} fusion(f32[2,16,4,256,256]{4,3,2,1,0:T(8,128)} %param.38, f32[16,4]{1,0:T(8,128)S(1)} %copy.242, bf16[16,4,8,256]{3,2,0,1:T(8,128)(2,1)S(1)} %get-tuple-element.27, bf16[4,16,8,256]{3,2,1,0:T(8,128)(2,1)S(1)} %copy-done.9), kind=kOutput, calls=%fused_computation.7 | convolution fusion | flops 75497472 | bytes 34078976 | tf_op jit(solution)/shard_map/bhs,bhsd,bhse->bhde/dot_general | solution.py:95
  236.0 10.8 %fusion.7 = f32[1,16,4,256,256]{4,3,2,1,0:T(8,128)} fusion(f32[2,16,4,256,256]{4,3,2,1,0:T(8,128)} %param.38, f32[16,4]{1,0:T(8,128)S(1)} %copy.234, bf16[16,4,8,256]{3,2,0,1:T(8,128)(2,1)S(1)} %get-tuple-element.25, bf16[4,16,8,256]{3,2,1,0:T(8,128)(2,1)S(1)} %copy-done.7), kind=kOutput, calls=%fused_computation.12 | convolution fusion | flops 75497472 | bytes 34078976 | tf_op jit(solution)/shard_map/bhs,bhsd,bhse->bhde/dot_general | solution.py:95
  246.8 3.0 %convolution_convert_fusion.4 = bf16[512,512]{1,0:T(8,128)(2,1)} fusion(bf16[64,8,1024]{2,1,0:T(8,128)(2,1)} %all-gather.5.cloned.1.call-done, bf16[2,1024,512]{2,1,0:T(8,128)(2,1)} %param.36), kind=kOutput, calls=%fused_computation.28 | convolution fusion | flops 537133056 | bytes 2621440 | tf_op jit(solution)/shard_map/dot_general | solution.py:170
  249.9 23.1 %pad_maximum_fusion = f32[2,16,4,256,256]{4,3,2,1,0:T(8,128)} fusion(f32[1,16,4,256,256]{4,3,2,1,0:T(8,128)} %fusion.3, f32[1,16,4,256,256]{4,3,2,1,0:T(8,128)} %fusion.7), kind=kLoop, calls=%fused_computation.2 | loop fusion | flops 8388608 | bytes 67108864 | tf_op jit(solution)/shard_map/stack | solution.py:242
  273.0 0.9 add_convert_fusion
  273.9 15.6 %all_gather.15 = bf16[512,512]{1,0:T(8,128)(2,1)S(1)} all-gather(bf16[128,512]{1,0:T(8,128)(2,1)S(1)} %add_convert_fusion), channel_id=1, replica_groups=mesh['grp'=2,'tp'=4,'dp'=4] {'tp'}, dimensions={0}, use_global_device_ids=true | all-gather | bytes 655360 | tf_op jit(solution)/shard_map/all_gather | solution.py:186
  289.5 0.8 copy.380
  (184 shorter events, 10.2 us)
Async XLA Ops:
  7.2 17.8 %copy-start = (bf16[64,8,512]{2,1,0:T(8,128)(2,1)S(1)}, bf16[64,8,512]{2,1,0:T(8,128)(2,1)}, u32[]{:S(2)}) copy-start(bf16[64,8,512]{2,1,0:T(8,128)(2,1)} %param.21) | copy-start | bytes 1572868
  7.2 17.8 %copy-start.47 = (bf16[2,512,1024]{2,1,0:T(8,128)(2,1)S(1)}, bf16[2,512,1024]{2,1,0:T(8,128)(2,1)}, u32[]{:S(2)}) copy-start(bf16[2,512,1024]{2,1,0:T(8,128)(2,1)} %param.24) | copy-start | bytes 6291460
  7.2 53.3 %reduce-scatter.15.cloned.1.call-start = ((), (), s32[]{:S(2)}) async-start(), calls=%async_computation.8 | async-start | bytes 2621440
  28.7 0.7 copy-start.45
  28.7 0.8 copy-start.24
  28.7 1.4 copy-start.43
  28.7 2.0 copy-start.44
  28.7 2.6 copy-start.32
  28.7 3.2 %copy-start.33 = (f32[2,1024]{1,0:T(2,128)S(1)}, f32[2,1024]{1,0:T(2,128)}, u32[]{:S(2)}) copy-start(f32[2,1024]{1,0:T(2,128)} %param.35) | copy-start | bytes 24580
  28.7 3.7 %copy-start.26 = (bf16[2,4,768]{2,1,0:T(4,128)(2,1)S(1)}, bf16[2,4,768]{2,1,0:T(4,128)(2,1)}, u32[]{:S(2)}) copy-start(bf16[2,4,768]{2,1,0:T(4,128)(2,1)} %param.30) | copy-start | bytes 36868
  28.7 4.3 %copy-start.27 = (bf16[2,4,768]{2,1,0:T(4,128)(2,1)S(1)}, bf16[2,4,768]{2,1,0:T(4,128)(2,1)}, u32[]{:S(2)}) copy-start(bf16[2,4,768]{2,1,0:T(4,128)(2,1)} %param.31) | copy-start | bytes 36868
  28.8 4.9 %copy-start.14 = (f32[2,4,1024]{2,1,0:T(4,128)S(1)}, f32[2,4,1024]{2,1,0:T(4,128)}, u32[]{:S(2)}) copy-start(f32[2,4,1024]{2,1,0:T(4,128)} %param.26) | copy-start | bytes 98308
  28.8 5.5 %copy-start.11 = (bf16[2,16,3,1024]{3,1,2,0:T(8,128)(2,1)S(1)}, bf16[2,16,3,1024]{3,1,2,0:T(8,128)(2,1)}, u32[]{:S(2)}) copy-start(bf16[2,16,3,1024]{3,1,2,0:T(8,128)(2,1)} %param.37) | copy-start | bytes 589828
  28.8 73.8 %all-gather.3.cloned.1.call-start = ((), (), s32[]{:S(2)}) async-start(), calls=%async_computation.4 | async-start | bytes 1310720 | tf_op jit(solution)/shard_map/all_gather | solution.py:168
  29.4 32.5 %copy-start.28 = (pred[16,8]{0,1:T(8,128)(4,1)}, pred[16,8]{0,1:T(8,128)(4,1)S(1)}, u32[]{:S(2)}) copy-start(pred[16,8]{0,1:T(8,128)(4,1)S(1)} %iota_compare_fusion.1) | copy-start | bytes 388
  30.1 42.2 %copy-start.39 = (pred[8,8]{1,0:T(8,128)(4,1)}, pred[8,8]{1,0:T(8,128)(4,1)S(1)}, u32[]{:S(2)}) copy-start(pred[8,8]{1,0:T(8,128)(4,1)S(1)} %iota_compare_fusion) | copy-start | bytes 196
  30.7 41.6 %copy-start.38 = (f32[4]{0:T(128)}, f32[4]{0:T(128)S(1)}, u32[]{:S(2)}) copy-start(f32[4]{0:T(128)S(1)} %get-tuple-element.66) | copy-start | bytes 52
  60.5 3.0 copy-start.3
  63.4 1.7 copy-start.10
  63.4 1.7 copy-start.48
  65.6 16.6 %copy-start.6 = (bf16[4,16,8,256]{3,2,1,0:T(8,128)(2,1)}, bf16[4,16,8,256]{3,2,1,0:T(8,128)(2,1)S(1)}, u32[]{:S(2)}) copy-start(bf16[4,16,8,256]{3,2,1,0:T(8,128)(2,1)S(1)} %convolution_convert_fusion.9) | copy-start | bytes 786436
  72.3 0.6 copy-start.12
  73.5 8.7 %copy-start.15 = (f32[16,4,1]{0,1,2:T(4,128)}, f32[16,4,1]{0,1,2:T(4,128)S(1)}, u32[]{:S(2)}) copy-start(f32[16,4,1]{0,1,2:T(4,128)S(1)} %copy.232) | copy-start | bytes 772
  75.2 7.0 %copy-start.13 = (f32[16,4,8]{2,1,0:T(4,128)S(1)}, f32[16,4,8]{2,1,0:T(4,128)}, u32[]{:S(2)}) copy-start(f32[16,4,8]{2,1,0:T(4,128)} %copy-done.12) | copy-start | bytes 6148
  82.2 1.8 copy-start.23
  83.6 0.7 copy-start.29
  85.7 41.9 %reduce-scatter.11.cloned.1.call-start = ((), (), s32[]{:S(2)}) async-start(), calls=%async_computation.5 | async-start | bytes 655360 | tf_op jit(solution)/shard_map/reduce_scatter | solution.py:173
  105.6 49.1 %copy-start.42 = (f32[1,512]{1,0:T(1,128)S(1)}, f32[1,512]{1,0:T(1,128)}, u32[]{:S(2)}) copy-start(f32[1,512]{1,0:T(1,128)} %get-tuple-element.60) | copy-start | bytes 6148
  105.6 86.0 %reduce-scatter.17.cloned.1.call-start = ((), (), s32[]{:S(2)}) async-start(), calls=%async_computation.9 | async-start | bytes 2621440
  161.7 0.7 copy-start.46
  161.7 1.3 copy-start.34
  161.7 85.1 %all-gather.5.cloned.1.call-start = ((), (), s32[]{:S(2)}) async-start(), calls=%async_computation.6 | async-start | bytes 1310720 | tf_op jit(solution)/shard_map/all_gather | solution.py:168
  191.6 3.2 %copy-start.17 = (f32[1,1,1024]{2,1,0:T(1,128)S(1)}, f32[1,1,1024]{2,1,0:T(1,128)}, u32[]{:S(2)}) copy-start(f32[1,1,1024]{2,1,0:T(1,128)} %get-tuple-element.37) | copy-start | bytes 12292
  191.6 3.2 %copy-start.18 = (f32[1,1,1024]{2,1,0:T(1,128)S(1)}, f32[1,1,1024]{2,1,0:T(1,128)}, u32[]{:S(2)}) copy-start(f32[1,1,1024]{2,1,0:T(1,128)} %get-tuple-element.38) | copy-start | bytes 12292
  191.6 3.2 %copy-start.19 = (f32[1,1,1024]{2,1,0:T(1,128)S(1)}, f32[1,1,1024]{2,1,0:T(1,128)}, u32[]{:S(2)}) copy-start(f32[1,1,1024]{2,1,0:T(1,128)} %get-tuple-element.43) | copy-start | bytes 12292
  191.6 3.2 %copy-start.20 = (f32[1,1,1024]{2,1,0:T(1,128)S(1)}, f32[1,1,1024]{2,1,0:T(1,128)}, u32[]{:S(2)}) copy-start(f32[1,1,1024]{2,1,0:T(1,128)} %get-tuple-element.44) | copy-start | bytes 12292
  195.1 4.6 %copy-start.35 = (bf16[4,768,1,1]{1,0,2,3:T(4,128)(2,1)S(1)}, bf16[4,768,1,1]{1,0,2,3:T(4,128)(2,1)}, u32[]{:S(2)}) copy-start(bf16[4,768,1,1]{1,0,2,3:T(4,128)(2,1)} %get-tuple-element.49) | copy-start | bytes 18436
  195.3 2.9 copy-start.49
  196.7 4.8 %copy-start.1 = (bf16[4,16,8,256]{3,2,1,0:T(8,128)(2,1)}, bf16[4,16,8,256]{3,2,1,0:T(8,128)(2,1)S(1)}, u32[]{:S(2)}) copy-start(bf16[4,16,8,256]{3,2,1,0:T(8,128)(2,1)S(1)} %convolution_convert_fusion.8) | copy-start | bytes 786436
  198.2 5.2 %copy-start.4 = (bf16[4,16,8,256]{3,2,1,0:T(8,128)(2,1)}, bf16[4,16,8,256]{3,2,1,0:T(8,128)(2,1)S(1)}, u32[]{:S(2)}) copy-start(bf16[4,16,8,256]{3,2,1,0:T(8,128)(2,1)S(1)} %convolution_convert_fusion.7) | copy-start | bytes 786436
  198.2 3.4 %copy-start.36 = (bf16[4,768,1,1]{1,0,2,3:T(4,128)(2,1)S(1)}, bf16[4,768,1,1]{1,0,2,3:T(4,128)(2,1)}, u32[]{:S(2)}) copy-start(bf16[4,768,1,1]{1,0,2,3:T(4,128)(2,1)} %get-tuple-element.47) | copy-start | bytes 18436
  199.7 3.7 %copy-start.8 = (bf16[4,16,8,256]{3,2,1,0:T(8,128)(2,1)}, bf16[4,16,8,256]{3,2,1,0:T(8,128)(2,1)S(1)}, u32[]{:S(2)}) copy-start(bf16[4,16,8,256]{3,2,1,0:T(8,128)(2,1)S(1)} %convolution_convert_fusion.6) | copy-start | bytes 786436
  199.7 3.7 %copy-start.41 = (f32[4]{0:T(128)S(1)}, f32[4]{0:T(128)}, u32[]{:S(2)}) copy-start(f32[4]{0:T(128)} %get-tuple-element.63) | copy-start | bytes 52
  199.7 6.7 %copy-start.37 = (f32[4]{0:T(128)S(1)}, f32[4]{0:T(128)}, u32[]{:S(2)}) copy-start(f32[4]{0:T(128)} %get-tuple-element.65) | copy-start | bytes 52
  199.8 6.7 %copy-start.40 = (pred[8,8]{1,0:T(8,128)(4,1)S(1)}, pred[8,8]{1,0:T(8,128)(4,1)}, u32[]{:S(2)}) copy-start(pred[8,8]{1,0:T(8,128)(4,1)} %copy-done.39) | copy-start | bytes 196
  214.1 2.6 copy-start.31
  214.1 4.1 %copy-start.16 = (f32[16,4,1]{0,1,2:T(4,128)S(1)}, f32[16,4,1]{0,1,2:T(4,128)}, u32[]{:S(2)}) copy-start(f32[16,4,1]{0,1,2:T(4,128)} %copy-done.15) | copy-start | bytes 772
  214.2 4.1 %copy-start.25 = (f32[2,16,4]{1,2,0:T(4,128)S(1)}, f32[2,16,4]{1,2,0:T(4,128)}, u32[]{:S(2)}) copy-start(f32[2,16,4]{1,2,0:T(4,128)} %param.39) | copy-start | bytes 1540
  215.4 5.0 %copy-start.2 = (bf16[4,16,8,256]{3,2,1,0:T(8,128)(2,1)S(1)}, bf16[4,16,8,256]{3,2,1,0:T(8,128)(2,1)}, u32[]{:S(2)}) copy-start(bf16[4,16,8,256]{3,2,1,0:T(8,128)(2,1)} %copy-done.1) | copy-start | bytes 786436
  220.4 1.9 copy-start.22
  221.9 1.0 copy-start.5
  221.9 0.9 copy-start.21
  221.9 0.9 copy-start.30
  222.3 2.8 copy-start.9
  224.3 48.7 %reduce-scatter.13.cloned.1.call-start = ((), (), s32[]{:S(2)}) async-start(), calls=%async_computation.7 | async-start | bytes 655360 | tf_op jit(solution)/shard_map/reduce_scatter | solution.py:173
  225.1 10.9 %copy-start.7 = (bf16[4,16,8,256]{3,2,1,0:T(8,128)(2,1)S(1)}, bf16[4,16,8,256]{3,2,1,0:T(8,128)(2,1)}, u32[]{:S(2)}) copy-start(bf16[4,16,8,256]{3,2,1,0:T(8,128)(2,1)} %copy-done.6) | copy-start | bytes 786436
Sparse Core Ops, SparseCore 0:
  28.9 31.4 reduce-scatter.14
  85.8 16.6 all-gather.2
  105.8 21.8 reduce-scatter.10
  161.9 29.7 reduce-scatter.16
  224.4 16.7 all-gather.4
  250.0 21.9 reduce-scatter.12
where the time goes:
time: 298 us; the launch traced here: 297 us
  waiting for transfers between devices  93 us (31%)
  matrix products  65.3 us (22%)
  blocking collectives  54.3 us (18%)
  other arithmetic  41.4 us (14%)
  local copies, waits for them, and re-layouts  27.7 us (9%)
  between operations  15 us (5%)
    unnamed x8, waiting for transfers between devices  54.4 us
    all_gather x2, blocking collectives, layer_step(): lax.all_gather(new_share, 'tp', axis=0, tiled=True)  31.1 us
    psum x2, blocking collectives, layer_step(): total_squares = lax.psum(partial_squares, 'dp')  23.2 us
    another operation x1, other arithmetic, per_device(): jnp.stack(memory_list)  23.1 us
    reduce_scatter x2, waiting for transfers between devices, layer_step(): lax.psum_scatter(flat_terms.astype(jnp.bfloat16), 'tp', scatter_dimension...  21.8 us
    dot_general x2, matrix products, recurrent_cell(): jnp.einsum('bhs,bhsd,bhse->bhde', update_weight, key_heads, value_heads)  21.7 us
    all_gather x2, waiting for transfers between devices, layer_step(): piece = lax.all_gather(mixed, 'dp', axis=0, tiled=True)  16.8 us
    dot_general x2, matrix products, recurrent_cell(): jnp.einsum('bhtd,bhde->bhte', query_heads, memory)  14 us
  transfers between devices with their start and end apart: 6, of which 4 were waited for; matrix products, arithmetic and copies ran while one was open for 17% of the time, Pallas kernels for 0%

commit v1 on v0

--- a/solution.py
+++ b/solution.py
@@ -130,7 +130,11 @@
     local_batch = live_counts.shape[0]
     floats = tokens.astype(jnp.float32)
     partial_squares = jnp.sum(floats * floats, axis=-1)
-    total_squares = lax.psum(partial_squares, "dp")
+    total_squares = partial_squares
+    for hop in (1, 2):
+        total_squares = total_squares + lax.ppermute(
+            total_squares, "dp", [(dev, dev ^ hop) for dev in range(4)]
+        )
     normed = (floats * lax.rsqrt(total_squares / D + epsilon)[..., None] * gain).astype(
         jnp.bfloat16
     )

time: 298 us -> 286 us (0.960)
  blocking collectives: 54.3 us -> 31.1 us
  waiting for transfers between devices: 93 us -> 99.3 us
  starting transfers between devices: 0.47 us -> 5.51 us
    psum x2 -> x0, blocking collectives: 23.2 us -> none  [layer_step(): total_squares = lax.psum(partial_squares, 'dp')]
    ppermute x0 -> x4, starting transfers between devices: none -> 5.04 us  [layer_step(): lax.ppermute(total_squares, 'dp', [(dev, dev ^ hop) for dev in range(4)])]
    ppermute x0 -> x4, waiting for transfers between devices: none -> 4.92 us  [layer_step(): lax.ppermute(total_squares, 'dp', [(dev, dev ^ hop) for dev in range(4)])]
  transfers between devices with their start and end apart: 6 -> 10, of which waited for: 4 -> 8; matrix products, arithmetic and copies ran while one was open for 17% -> 18% of each run, Pallas kernels for 0% -> 0%
where the time goes in v1:
time: 286 us; the launch traced here: 285 us
  waiting for transfers between devices  99.3 us (35%)
  matrix products  65.4 us (23%)
  other arithmetic  41.5 us (15%)
  blocking collectives  31.1 us (11%)
  local copies, waits for them, and re-layouts  27.5 us (10%)
  between operations  15 us (5%)
  starting transfers between devices  5.51 us (2%)
    unnamed x8, waiting for transfers between devices  55.8 us
    all_gather x2, blocking collectives, layer_step(): lax.all_gather(new_share, 'tp', axis=0, tiled=True)  31.1 us
    another operation x1, other arithmetic, per_device(): jnp.stack(memory_list)  23.1 us
    reduce_scatter x2, waiting for transfers between devices, layer_step(): lax.psum_scatter(flat_terms.astype(jnp.bfloat16), 'tp', scatter_dimension...  21.8 us
    dot_general x2, matrix products, recurrent_cell(): jnp.einsum('bhs,bhsd,bhse->bhde', update_weight, key_heads, value_heads)  21.7 us
    all_gather x2, waiting for transfers between devices, layer_step(): piece = lax.all_gather(mixed, 'dp', axis=0, tiled=True)  16.8 us
    dot_general x2, matrix products, recurrent_cell(): jnp.einsum('bhtd,bhde->bhte', query_heads, memory)  14 us
    unnamed x110, local copies, waits for them, and re-layouts  11.9 us
  transfers between devices with their start and end apart: 10, of which 8 were waited for; matrix products, arithmetic and copies ran while one was open for 18% of the time, Pallas kernels for 0%

profile of v1, /device:TPU:0, one launch (start us, length us, event | category | flops | bytes accessed | tf_op | source)
XLA Modules:
  0.0 285.3 jit_solution(6040385288834833798)
XLA Ops:
  7.2 1.4 fusion.16
  8.6 0.6 collective-permute-start
  9.2 0.9 collective-permute-done
  10.0 2.8 collective-permute-start.1
  12.8 1.3 fusion.162
  14.8 2.1 fusion.11
  16.9 0.8 fusion.10
  18.1 2.5 copy.279
  21.4 0.6 slice_bitcast_fusion.8
  23.1 0.6 slice_bitcast_fusion.6
  23.7 0.6 fusion.161
  24.3 0.6 slice_bitcast_fusion.2
  24.9 0.6 slice_bitcast_fusion.3
  25.5 0.6 fusion.160
  26.1 27.7 %reduce-scatter.15.cloned.1.call-done = bf16[16,16384]{1,0:T(8,128)(2,1)} async-done(((bf16[64,16384]{1,0:T(8,128)(2,1)}), bf16[16,16384]{1,0:T(8,128)(2,1)}) %reduce-scatter.15.cloned.1.call-update) | async-done | bytes 524304
  53.9 1.4 copy.280
  55.5 0.9 reshape.308
  57.1 1.4 convolution_convert_fusion.10
  59.0 1.8 fusion.76
  60.9 1.8 fusion.77
  62.8 2.8 reduce_window_sum.17
  67.0 0.8 exponential_multiply_fusion.1
  67.8 0.8 bitcast_multiply_fusion.6
  68.6 7.0 %fusion.4 = f32[16,4,8,256]{3,2,1,0:T(8,128)S(1)} fusion(f32[2,16,4,256,256]{4,3,2,1,0:T(8,128)} %param.38, bf16[4,16,8,256]{3,2,1,0:T(8,128)(2,1)S(1)} %convolution_convert_fusion.11), kind=kOutput, calls=%fused_computation.9 | convolution fusion | flops 67108864 | bytes 9175040 | tf_op jit(solution)/shard_map/bhtd,bhde->bhte/dot_general | solution.py:83
  75.6 1.4 fusion.108
  78.2 0.9 copy.214
  79.2 16.8 %all-gather.3.cloned.1.call-done = bf16[64,8,1024]{2,1,0:T(8,128)(2,1)} async-done(((bf16[16,8,1024]{2,1,0:T(8,128)(2,1)}), bf16[64,8,1024]{2,1,0:T(8,128)(2,1)}) %all-gather.3.cloned.1.call-update) | async-done | bytes 1048592 | tf_op jit(solution)/shard_map/all_gather | solution.py:172
  96.0 3.0 %convolution_convert_fusion.5 = bf16[512,512]{1,0:T(8,128)(2,1)} fusion(bf16[64,8,1024]{2,1,0:T(8,128)(2,1)} %all-gather.3.cloned.1.call-done, bf16[2,1024,512]{2,1,0:T(8,128)(2,1)} %param.36), kind=kOutput, calls=%fused_computation.29 | convolution fusion | flops 537133056 | bytes 2621440 | tf_op jit(solution)/shard_map/dot_general | solution.py:174
  99.2 21.8 %reduce-scatter.11.cloned.1.call-done = bf16[128,512]{1,0:T(8,128)(2,1)} async-done(((bf16[512,512]{1,0:T(8,128)(2,1)}), bf16[128,512]{1,0:T(8,128)(2,1)}) %reduce-scatter.11.cloned.1.call-update) | async-done | bytes 131088 | tf_op jit(solution)/shard_map/reduce_scatter | solution.py:177
  121.0 0.9 add_convert_fusion.1
  121.9 15.6 %all_gather.13 = bf16[512,512]{1,0:T(8,128)(2,1)S(1)} all-gather(bf16[128,512]{1,0:T(8,128)(2,1)S(1)} %add_convert_fusion.1), channel_id=1, replica_groups=mesh['grp'=2,'tp'=4,'dp'=4] {'tp'}, dimensions={0}, use_global_device_ids=true | all-gather | bytes 655360 | tf_op jit(solution)/shard_map/all_gather | solution.py:190
  137.8 1.2 collective-permute-done.2
  139.0 1.6 collective-permute-start.3
  140.6 2.3 collective-permute-done.3
  143.1 2.0 fusion.13
  145.1 2.0 fusion.12
  147.5 2.5 copy.281
  150.1 0.6 copy-done.46
  150.7 0.7 copy.228
  151.8 28.0 %reduce-scatter.17.cloned.1.call-done = bf16[16,16384]{1,0:T(8,128)(2,1)} async-done(((bf16[64,16384]{1,0:T(8,128)(2,1)}), bf16[16,16384]{1,0:T(8,128)(2,1)}) %reduce-scatter.17.cloned.1.call-update) | async-done | bytes 524304
  179.8 1.4 copy.282
  181.1 0.7 fusion.158
  182.0 0.9 reshape.309
  183.5 1.4 convolution_convert_fusion.8
  184.9 1.4 convolution_convert_fusion.7
  186.4 1.5 convolution_convert_fusion.6
  187.9 1.8 fusion.74
  189.7 1.8 fusion.75
  191.7 2.8 reduce_window_sum.18
  195.2 7.1 %fusion = f32[16,4,8,256]{3,2,1,0:T(8,128)S(1)} fusion(f32[2,16,4,256,256]{4,3,2,1,0:T(8,128)} %param.38, bf16[4,16,8,256]{3,2,1,0:T(8,128)(2,1)} %copy-done.1), kind=kOutput, calls=%fused_computation.4 | convolution fusion | flops 67108864 | bytes 9175040 | tf_op jit(solution)/shard_map/bhtd,bhde->bhte/dot_general | solution.py:83
  202.3 1.2 gather_fusion
  203.5 1.2 gather_fusion.1
  205.3 0.8 copy.250
  206.8 1.7 bitcast_multiply_fusion.3
  208.6 1.5 fusion.109
  211.5 0.9 copy.227
  212.7 0.6 pad_maximum_fusion.12
  213.3 10.9 %fusion.3 = f32[1,16,4,256,256]{4,3,2,1,0:T(8,128)} fusion(f32[2,16,4,256,256]{4,3,2,1,0:T(8,128)} %param.38, f32[16,4]{1,0:T(8,128)S(1)} %copy.242, bf16[16,4,8,256]{3,2,0,1:T(8,128)(2,1)S(1)} %get-tuple-element.27, bf16[4,16,8,256]{3,2,1,0:T(8,128)(2,1)S(1)} %copy-done.9), kind=kOutput, calls=%fused_computation.7 | convolution fusion | flops 75497472 | bytes 34078976 | tf_op jit(solution)/shard_map/bhs,bhsd,bhse->bhde/dot_general | solution.py:95
  224.2 10.9 %fusion.7 = f32[1,16,4,256,256]{4,3,2,1,0:T(8,128)} fusion(f32[2,16,4,256,256]{4,3,2,1,0:T(8,128)} %param.38, f32[16,4]{1,0:T(8,128)S(1)} %copy.234, bf16[16,4,8,256]{3,2,0,1:T(8,128)(2,1)S(1)} %get-tuple-element.25, bf16[4,16,8,256]{3,2,1,0:T(8,128)(2,1)S(1)} %copy-done.7), kind=kOutput, calls=%fused_computation.12 | convolution fusion | flops 75497472 | bytes 34078976 | tf_op jit(solution)/shard_map/bhs,bhsd,bhse->bhde/dot_general | solution.py:95
  235.0 3.0 %convolution_convert_fusion.4 = bf16[512,512]{1,0:T(8,128)(2,1)} fusion(bf16[64,8,1024]{2,1,0:T(8,128)(2,1)} %all-gather.5.cloned.1.call-done, bf16[2,1024,512]{2,1,0:T(8,128)(2,1)} %param.36), kind=kOutput, calls=%fused_computation.28 | convolution fusion | flops 537133056 | bytes 2621440 | tf_op jit(solution)/shard_map/dot_general | solution.py:174
  238.1 23.1 %pad_maximum_fusion = f32[2,16,4,256,256]{4,3,2,1,0:T(8,128)} fusion(f32[1,16,4,256,256]{4,3,2,1,0:T(8,128)} %fusion.3, f32[1,16,4,256,256]{4,3,2,1,0:T(8,128)} %fusion.7), kind=kLoop, calls=%fused_computation.2 | loop fusion | flops 8388608 | bytes 67108864 | tf_op jit(solution)/shard_map/stack | solution.py:246
  261.2 0.9 add_convert_fusion
  262.1 15.5 %all_gather.15 = bf16[512,512]{1,0:T(8,128)(2,1)S(1)} all-gather(bf16[128,512]{1,0:T(8,128)(2,1)S(1)} %add_convert_fusion), channel_id=1, replica_groups=mesh['grp'=2,'tp'=4,'dp'=4] {'tp'}, dimensions={0}, use_global_device_ids=true | all-gather | bytes 655360 | tf_op jit(solution)/shard_map/all_gather | solution.py:190
  277.6 0.8 copy.380
  (192 shorter events, 12.9 us)
Async XLA Ops:
  7.2 9.7 %copy-start = (bf16[64,8,512]{2,1,0:T(8,128)(2,1)S(1)}, bf16[64,8,512]{2,1,0:T(8,128)(2,1)}, u32[]{:S(2)}) copy-start(bf16[64,8,512]{2,1,0:T(8,128)(2,1)} %param.21) | copy-start | bytes 1572868
  7.2 9.7 %copy-start.47 = (bf16[2,512,1024]{2,1,0:T(8,128)(2,1)S(1)}, bf16[2,512,1024]{2,1,0:T(8,128)(2,1)}, u32[]{:S(2)}) copy-start(bf16[2,512,1024]{2,1,0:T(8,128)(2,1)} %param.24) | copy-start | bytes 6291460
  7.2 46.7 %reduce-scatter.15.cloned.1.call-start = ((), (), s32[]{:S(2)}) async-start(), calls=%async_computation.8 | async-start | bytes 2621440
  8.6 1.4 collective-permute-start
  10.0 4.7 %collective-permute-start.1 = (f32[64,8]{1,0:T(8,128)S(1)}, f32[64,8]{1,0:T(8,128)S(1)}, u32[]{:S(2)}, u32[]{:S(2)}) collective-permute-start(f32[64,8]{1,0:T(8,128)S(1)} %add.281), channel_id=1, source_target_pairs={{0,2},{1,3},{2,0},{3,1},{4,6},{5,7},{6,4},{7,5},{8,10},{9,11},{10,... | collective-permute-start | bytes 6152 | tf_op jit(solution)/shard_map/ppermute | solution.py:135
  20.7 0.7 copy-start.45
  20.7 0.8 copy-start.24
  20.7 1.4 copy-start.43
  20.7 2.0 copy-start.44
  20.7 2.4 copy-start.32
  20.7 3.0 %copy-start.33 = (f32[2,1024]{1,0:T(2,128)S(1)}, f32[2,1024]{1,0:T(2,128)}, u32[]{:S(2)}) copy-start(f32[2,1024]{1,0:T(2,128)} %param.35) | copy-start | bytes 24580
  20.7 3.6 %copy-start.26 = (bf16[2,4,768]{2,1,0:T(4,128)(2,1)S(1)}, bf16[2,4,768]{2,1,0:T(4,128)(2,1)}, u32[]{:S(2)}) copy-start(bf16[2,4,768]{2,1,0:T(4,128)(2,1)} %param.30) | copy-start | bytes 36868
  20.7 4.2 %copy-start.27 = (bf16[2,4,768]{2,1,0:T(4,128)(2,1)S(1)}, bf16[2,4,768]{2,1,0:T(4,128)(2,1)}, u32[]{:S(2)}) copy-start(bf16[2,4,768]{2,1,0:T(4,128)(2,1)} %param.31) | copy-start | bytes 36868
  20.7 4.8 %copy-start.14 = (f32[2,4,1024]{2,1,0:T(4,128)S(1)}, f32[2,4,1024]{2,1,0:T(4,128)}, u32[]{:S(2)}) copy-start(f32[2,4,1024]{2,1,0:T(4,128)} %param.26) | copy-start | bytes 98308
  20.7 5.4 %copy-start.11 = (bf16[2,16,3,1024]{3,1,2,0:T(8,128)(2,1)S(1)}, bf16[2,16,3,1024]{3,1,2,0:T(8,128)(2,1)}, u32[]{:S(2)}) copy-start(bf16[2,16,3,1024]{3,1,2,0:T(8,128)(2,1)} %param.37) | copy-start | bytes 589828
  20.8 75.2 %all-gather.3.cloned.1.call-start = ((), (), s32[]{:S(2)}) async-start(), calls=%async_computation.4 | async-start | bytes 1310720 | tf_op jit(solution)/shard_map/all_gather | solution.py:172
  21.3 34.0 %copy-start.28 = (pred[16,8]{0,1:T(8,128)(4,1)}, pred[16,8]{0,1:T(8,128)(4,1)S(1)}, u32[]{:S(2)}) copy-start(pred[16,8]{0,1:T(8,128)(4,1)S(1)} %iota_compare_fusion.1) | copy-start | bytes 388
  22.1 43.7 %copy-start.39 = (pred[8,8]{1,0:T(8,128)(4,1)}, pred[8,8]{1,0:T(8,128)(4,1)S(1)}, u32[]{:S(2)}) copy-start(pred[8,8]{1,0:T(8,128)(4,1)S(1)} %iota_compare_fusion) | copy-start | bytes 196
  22.6 43.1 %copy-start.38 = (f32[4]{0:T(128)}, f32[4]{0:T(128)S(1)}, u32[]{:S(2)}) copy-start(f32[4]{0:T(128)S(1)} %get-tuple-element.66) | copy-start | bytes 52
  53.9 3.0 %copy-start.3 = (bf16[2,4,256,256]{3,2,1,0:T(8,128)(2,1)S(1)}, bf16[2,4,256,256]{3,2,1,0:T(8,128)(2,1)}, u32[]{:S(2)}) copy-start(bf16[2,4,256,256]{3,2,1,0:T(8,128)(2,1)} %param.27) | copy-start | bytes 3145732
  56.8 1.7 copy-start.10
  56.8 1.7 copy-start.48
  59.0 16.6 %copy-start.6 = (bf16[4,16,8,256]{3,2,1,0:T(8,128)(2,1)}, bf16[4,16,8,256]{3,2,1,0:T(8,128)(2,1)S(1)}, u32[]{:S(2)}) copy-start(bf16[4,16,8,256]{3,2,1,0:T(8,128)(2,1)S(1)} %convolution_convert_fusion.9) | copy-start | bytes 786436
  65.8 0.6 copy-start.12
  66.9 8.6 %copy-start.15 = (f32[16,4,1]{0,1,2:T(4,128)}, f32[16,4,1]{0,1,2:T(4,128)S(1)}, u32[]{:S(2)}) copy-start(f32[16,4,1]{0,1,2:T(4,128)S(1)} %copy.232) | copy-start | bytes 772
  68.6 7.0 %copy-start.13 = (f32[16,4,8]{2,1,0:T(4,128)S(1)}, f32[16,4,8]{2,1,0:T(4,128)}, u32[]{:S(2)}) copy-start(f32[16,4,8]{2,1,0:T(4,128)} %copy-done.12) | copy-start | bytes 6148
  75.6 1.8 copy-start.23
  77.0 0.7 copy-start.29
  79.1 41.9 %reduce-scatter.11.cloned.1.call-start = ((), (), s32[]{:S(2)}) async-start(), calls=%async_computation.5 | async-start | bytes 655360 | tf_op jit(solution)/shard_map/reduce_scatter | solution.py:177
  99.0 44.1 %copy-start.42 = (f32[1,512]{1,0:T(1,128)S(1)}, f32[1,512]{1,0:T(1,128)}, u32[]{:S(2)}) copy-start(f32[1,512]{1,0:T(1,128)} %get-tuple-element.60) | copy-start | bytes 6148
  99.0 80.8 %reduce-scatter.17.cloned.1.call-start = ((), (), s32[]{:S(2)}) async-start(), calls=%async_computation.9 | async-start | bytes 2621440
  137.8 1.3 collective-permute-start.2
  139.0 3.9 %collective-permute-start.3 = (f32[64,8]{1,0:T(8,128)S(1)}, f32[64,8]{1,0:T(8,128)S(1)}, u32[]{:S(2)}, u32[]{:S(2)}) collective-permute-start(f32[64,8]{1,0:T(8,128)S(1)} %add.307), channel_id=1, source_target_pairs={{0,2},{1,3},{2,0},{3,1},{4,6},{5,7},{6,4},{7,5},{8,10},{9,11},{10,... | collective-permute-start | bytes 6152 | tf_op jit(solution)/shard_map/ppermute | solution.py:135
  150.0 0.7 copy-start.46
  150.0 1.3 copy-start.34
  150.0 85.0 %all-gather.5.cloned.1.call-start = ((), (), s32[]{:S(2)}) async-start(), calls=%async_computation.6 | async-start | bytes 1310720 | tf_op jit(solution)/shard_map/all_gather | solution.py:172
  179.8 3.2 %copy-start.17 = (f32[1,1,1024]{2,1,0:T(1,128)S(1)}, f32[1,1,1024]{2,1,0:T(1,128)}, u32[]{:S(2)}) copy-start(f32[1,1,1024]{2,1,0:T(1,128)} %get-tuple-element.37) | copy-start | bytes 12292
  179.8 3.2 %copy-start.18 = (f32[1,1,1024]{2,1,0:T(1,128)S(1)}, f32[1,1,1024]{2,1,0:T(1,128)}, u32[]{:S(2)}) copy-start(f32[1,1,1024]{2,1,0:T(1,128)} %get-tuple-element.38) | copy-start | bytes 12292
  179.8 3.2 %copy-start.19 = (f32[1,1,1024]{2,1,0:T(1,128)S(1)}, f32[1,1,1024]{2,1,0:T(1,128)}, u32[]{:S(2)}) copy-start(f32[1,1,1024]{2,1,0:T(1,128)} %get-tuple-element.43) | copy-start | bytes 12292
  179.8 3.2 %copy-start.20 = (f32[1,1,1024]{2,1,0:T(1,128)S(1)}, f32[1,1,1024]{2,1,0:T(1,128)}, u32[]{:S(2)}) copy-start(f32[1,1,1024]{2,1,0:T(1,128)} %get-tuple-element.44) | copy-start | bytes 12292
  183.3 4.6 %copy-start.35 = (bf16[4,768,1,1]{1,0,2,3:T(4,128)(2,1)S(1)}, bf16[4,768,1,1]{1,0,2,3:T(4,128)(2,1)}, u32[]{:S(2)}) copy-start(bf16[4,768,1,1]{1,0,2,3:T(4,128)(2,1)} %get-tuple-element.49) | copy-start | bytes 18436
  183.5 2.9 %copy-start.49 = (bf16[2,4,256,256]{3,2,1,0:T(8,128)(2,1)S(1)}, bf16[2,4,256,256]{3,2,1,0:T(8,128)(2,1)}, u32[]{:S(2)}) copy-start(bf16[2,4,256,256]{3,2,1,0:T(8,128)(2,1)} %param.29) | copy-start | bytes 3145732
  184.9 4.8 %copy-start.1 = (bf16[4,16,8,256]{3,2,1,0:T(8,128)(2,1)}, bf16[4,16,8,256]{3,2,1,0:T(8,128)(2,1)S(1)}, u32[]{:S(2)}) copy-start(bf16[4,16,8,256]{3,2,1,0:T(8,128)(2,1)S(1)} %convolution_convert_fusion.8) | copy-start | bytes 786436
  186.4 5.2 %copy-start.4 = (bf16[4,16,8,256]{3,2,1,0:T(8,128)(2,1)}, bf16[4,16,8,256]{3,2,1,0:T(8,128)(2,1)S(1)}, u32[]{:S(2)}) copy-start(bf16[4,16,8,256]{3,2,1,0:T(8,128)(2,1)S(1)} %convolution_convert_fusion.7) | copy-start | bytes 786436
  186.4 3.4 %copy-start.36 = (bf16[4,768,1,1]{1,0,2,3:T(4,128)(2,1)S(1)}, bf16[4,768,1,1]{1,0,2,3:T(4,128)(2,1)}, u32[]{:S(2)}) copy-start(bf16[4,768,1,1]{1,0,2,3:T(4,128)(2,1)} %get-tuple-element.47) | copy-start | bytes 18436
  187.9 3.7 %copy-start.8 = (bf16[4,16,8,256]{3,2,1,0:T(8,128)(2,1)}, bf16[4,16,8,256]{3,2,1,0:T(8,128)(2,1)S(1)}, u32[]{:S(2)}) copy-start(bf16[4,16,8,256]{3,2,1,0:T(8,128)(2,1)S(1)} %convolution_convert_fusion.6) | copy-start | bytes 786436
  187.9 3.7 %copy-start.41 = (f32[4]{0:T(128)S(1)}, f32[4]{0:T(128)}, u32[]{:S(2)}) copy-start(f32[4]{0:T(128)} %get-tuple-element.63) | copy-start | bytes 52
  187.9 6.7 %copy-start.37 = (f32[4]{0:T(128)S(1)}, f32[4]{0:T(128)}, u32[]{:S(2)}) copy-start(f32[4]{0:T(128)} %get-tuple-element.65) | copy-start | bytes 52
  187.9 6.7 %copy-start.40 = (pred[8,8]{1,0:T(8,128)(4,1)S(1)}, pred[8,8]{1,0:T(8,128)(4,1)}, u32[]{:S(2)}) copy-start(pred[8,8]{1,0:T(8,128)(4,1)} %copy-done.39) | copy-start | bytes 196
  202.3 2.6 copy-start.31
  202.3 4.1 %copy-start.16 = (f32[16,4,1]{0,1,2:T(4,128)S(1)}, f32[16,4,1]{0,1,2:T(4,128)}, u32[]{:S(2)}) copy-start(f32[16,4,1]{0,1,2:T(4,128)} %copy-done.15) | copy-start | bytes 772
  202.3 4.1 %copy-start.25 = (f32[2,16,4]{1,2,0:T(4,128)S(1)}, f32[2,16,4]{1,2,0:T(4,128)}, u32[]{:S(2)}) copy-start(f32[2,16,4]{1,2,0:T(4,128)} %param.39) | copy-start | bytes 1540
  203.5 5.0 %copy-start.2 = (bf16[4,16,8,256]{3,2,1,0:T(8,128)(2,1)S(1)}, bf16[4,16,8,256]{3,2,1,0:T(8,128)(2,1)}, u32[]{:S(2)}) copy-start(bf16[4,16,8,256]{3,2,1,0:T(8,128)(2,1)} %copy-done.1) | copy-start | bytes 786436
  208.6 1.9 copy-start.22
  210.1 1.0 copy-start.5
  210.1 0.9 copy-start.21
  210.1 0.9 copy-start.30
  210.5 2.8 copy-start.9
  212.4 48.8 %reduce-scatter.13.cloned.1.call-start = ((), (), s32[]{:S(2)}) async-start(), calls=%async_computation.7 | async-start | bytes 655360 | tf_op jit(solution)/shard_map/reduce_scatter | solution.py:177
  213.3 10.9 %copy-start.7 = (bf16[4,16,8,256]{3,2,1,0:T(8,128)(2,1)S(1)}, bf16[4,16,8,256]{3,2,1,0:T(8,128)(2,1)}, u32[]{:S(2)}) copy-start(bf16[4,16,8,256]{3,2,1,0:T(8,128)(2,1)} %copy-done.6) | copy-start | bytes 786436
Sparse Core Ops, SparseCore 0:
  20.9 32.9 reduce-scatter.14
  79.2 16.6 all-gather.2
  99.2 21.8 reduce-scatter.10
  150.2 29.5 reduce-scatter.16
  212.5 16.7 all-gather.4
  238.2 21.9 reduce-scatter.12
